TPU v7x, 512 devices: a whole 4x4x16 slice. The times are simulated.
512 devices in a mesh: sp: 64 (over z, y), tp: 8 (over x, core).
Axes of the slice: x: 4, y: 4, z: 16, core: 2. Of those that a mesh axis runs over, the one named last changes fastest.
Arguments:
- queries: bfloat16 [32768, 1024], P('sp', 'tp'), may hold values from -8 to 8
- key_rows: bfloat16 [32768, 512], P('sp', 'tp'), may hold values from -8 to 8
- values: bfloat16 [32768, 512], P('sp', 'tp'), may hold values from -16 to 16
- doc_ids: int32 [32768], P('sp'), may hold values from 0 to 31, never falling along the last dimension, each value on 1 to 2048 neighbouring positions
- sink_logits: float32 [16], P('tp'), may hold values from 2.5 to 6
- residual: bfloat16 [32768, 2048], P('sp'), may hold values from -6 to 6
- out_weight: bfloat16 [1024, 2048], P('tp'), may hold values from -0.1875 to 0.1875
- norm_gain: float32 [2048], replicated, may hold values from 0.1 to 1.9
- w_gate: bfloat16 [2048, 5632], P('sp', 'tp'), may hold values from -0.125 to 0.125
- w_up: bfloat16 [2048, 5632], P('sp', 'tp'), may hold values from -0.125 to 0.125
- w_down: bfloat16 [5632, 2048], P('tp', 'sp'), may hold values from -0.078125 to 0.078125
Outputs:
- layer_out: bfloat16 [32768, 2048], P('sp')
Inputs may be any that keep to these rules, and one draw needn't show every extreme that they name: `doc_ids`: document numbers never fall along the positions; each document has 1 to 2048 positions.
All inputs are finite; a program needn't handle non-finite values.
Results may differ from a plain program's by a relative error of at most 0.014.
Values may be sent and summed in bfloat16 or wider, within the bound.
No kernel may reach another device: no remote copies, remote signals or barrier semaphores. Data moves between devices by JAX's collectives and lax.ppermute only.
A program may use at most 64 MiB of HBM per device.

v0:
```python
import jax
import jax.numpy as jnp
from jax import lax
from jax.sharding import PartitionSpec as P

HD = 64
WINDOW = 128


def from_behind(shard, axis, by):
    size = lax.axis_size(axis)
    pairs = [(i, i + by) for i in range(size) if 0 <= i + by < size]
    return lax.ppermute(shard, axis, pairs)


def gather_turned(arrays, axis, dims):
    turned = [jnp.moveaxis(a, dim, 0) for a, dim in zip(arrays, dims)]
    both = jnp.concatenate([t.reshape(len(t), -1) for t in turned], axis=1)
    result, at, finished = (lax.all_gather(both, axis, axis=0, tiled=True), 0, [])
    for t, dim in zip(turned, dims):
        slab = result[:, at : at + t[0].size].reshape(-1, *t.shape[1:])
        finished.append(jnp.moveaxis(slab, 0, dim))
        at += t[0].size
    return tuple(finished)


def cut_along(shard, dim, size):
    before, after = (shard.shape[:dim], shard.shape[dim + 1 :])
    return jnp.moveaxis(shard.reshape(*before, size, -1, *after), dim, 0)


def sum_at_owner(shard, axis, dim):
    pieces = cut_along(shard, dim, lax.axis_size(axis))
    arrived = lax.all_to_all(pieces, axis, split_axis=0, concat_axis=0, tiled=True)
    return arrived.astype(jnp.float32).sum(axis=0)


def laid_out(pieces, dim):
    dims = list(pieces.shape[1:])
    dims[dim] *= pieces.shape[0]
    return jnp.moveaxis(pieces, 0, dim).reshape(dims)


def sent_to_all(shard, axis):
    size = lax.axis_size(axis)
    return lax.all_to_all(
        jnp.broadcast_to(shard[None], (size, *shard.shape)), axis, 0, 0, tiled=True
    )


def gathered_copies(shard, axis, dim):
    return laid_out(sent_to_all(shard, axis), dim)


def rms_norm(stream, norm_gain):
    floats = stream.astype(jnp.float32)
    scale = lax.rsqrt(jnp.mean(floats * floats, axis=-1, keepdims=True) + 1e-06)
    return floats * scale * norm_gain


def band_rows(tensor, blocks):
    tensor = tensor.reshape((blocks + 1, WINDOW) + tensor.shape[1:])
    return jnp.concatenate([tensor[:-1], tensor[1:]], axis=1)


def attend(queries, key_rows, values, doc_ids, sink_logits):
    local_rows = queries.shape[0]
    blocks = local_rows // WINDOW
    kv_local = key_rows.shape[1] // HD
    per_kv = queries.shape[1] // key_rows.shape[1]
    tail_docs = doc_ids[local_rows - WINDOW :] + 1
    prev_keys, prev_values, prev_docs = from_behind(
        (key_rows[local_rows - WINDOW :], values[local_rows - WINDOW :], tail_docs), "sp", 1
    )
    key_band = band_rows(jnp.concatenate([prev_keys, key_rows], axis=0), blocks).reshape(
        blocks, 2 * WINDOW, kv_local, HD
    )
    value_band = band_rows(jnp.concatenate([prev_values, values], axis=0), blocks).reshape(
        blocks, 2 * WINDOW, kv_local, HD
    )
    doc_band = band_rows(jnp.concatenate([prev_docs - 1, doc_ids]), blocks)
    query_band = queries.reshape(blocks, WINDOW, kv_local, per_kv, HD)
    scores = jnp.einsum(
        "nqhgd,nkhd->nhgqk", query_band, key_band, preferred_element_type=jnp.float32
    ) * HD ** (-0.5)
    offsets = jnp.arange(WINDOW)[:, None] + WINDOW - jnp.arange(2 * WINDOW)[None, :]
    inside = (offsets >= 0) & (offsets < WINDOW)
    query_docs = doc_ids.reshape(blocks, WINDOW)
    allowed = inside[None] & (query_docs[:, :, None] == doc_band[:, None, :])
    scores = jnp.where(allowed[:, None, None], scores, -1e30)
    sink_logit = sink_logits.reshape(kv_local, per_kv)[None, :, :, None, None]
    peak = jnp.maximum(jnp.max(scores, axis=-1, keepdims=True), sink_logit)
    raised = jnp.exp(scores - peak)
    denom = jnp.sum(raised, axis=-1, keepdims=True) + jnp.exp(sink_logit - peak)
    weights = (raised / denom).astype(jnp.bfloat16)
    attended = jnp.einsum(
        "nhgqk,nkhd->nqhgd", weights, value_band, preferred_element_type=jnp.float32
    )
    return attended.astype(jnp.bfloat16).reshape(local_rows, queries.shape[1])


def on_device(
    queries,
    key_rows,
    values,
    doc_ids,
    sink_logits,
    residual,
    out_weight,
    norm_gain,
    w_gate,
    w_up,
    w_down,
):
    gate_whole, up_whole, down_whole = gather_turned((w_gate, w_up, w_down), "sp", (0, 0, 1))
    attended = attend(queries, key_rows, values, doc_ids, sink_logits)
    row_share = residual.shape[0] // lax.axis_size("tp")
    picked = attended
    mixed_sum = sum_at_owner(
        jnp.dot(picked, out_weight, preferred_element_type=jnp.float32).astype(jnp.bfloat16),
        "tp",
        0,
    )
    base_rows = lax.dynamic_slice_in_dim(residual, lax.axis_index("tp") * row_share, row_share, 0)
    stream = (base_rows.astype(jnp.float32) + mixed_sum).astype(jnp.bfloat16)
    normed = rms_norm(stream, norm_gain).astype(jnp.bfloat16)
    normed = gathered_copies(normed, "tp", 0)
    gate_act = jnp.dot(normed, gate_whole, preferred_element_type=jnp.float32)
    up_act = jnp.dot(normed, up_whole, preferred_element_type=jnp.float32)
    hidden = (jax.nn.silu(gate_act) * up_act).astype(jnp.bfloat16)
    picked = hidden
    mlp_total = sum_at_owner(
        jnp.dot(picked, down_whole, preferred_element_type=jnp.float32).astype(jnp.bfloat16),
        "tp",
        0,
    )
    finished = (stream.astype(jnp.float32) + mlp_total).astype(jnp.bfloat16)
    return gathered_copies(finished, "tp", 0)


def solution(mesh):
    in_specs = (
        P("sp", "tp"),
        P("sp", "tp"),
        P("sp", "tp"),
        P("sp"),
        P("tp"),
        P("sp", None),
        P("tp", None),
        P(),
        P("sp", "tp"),
        P("sp", "tp"),
        P("tp", "sp"),
    )
    out_specs = P("sp", None)
    return jax.shard_map(
        on_device, mesh=mesh, in_specs=in_specs, out_specs=out_specs, check_vma=False
    )
```

profile of v0, /device:TPU:1, one launch (start us, length us, event | category | flops | bytes accessed | tf_op | source)
XLA Modules:
  0.0 256.9 jit_solution(4028181509367564481)
XLA Ops:
  6.5 1.7 concatenate.27
  8.9 4.0 %collective-permute-start.1 = (s32[128]{0:T(128)S(1)}, s32[128]{0:T(128)S(1)}, u32[]{:S(2)}, u32[]{:S(2)}) collective-permute-start(s32[128]{0:T(128)S(1)} %slice_add_fusion), channel_id=1, source_target_pairs={{0,8},{8,16},{16,24},{24,32},{32,40},{40,48},{48,56},{56,64},{64,7... | collective-permute-start | bytes 1544 | tf_op jit(solution)/shard_map/ppermute | solution.py:13
  12.9 0.7 slice.56
  13.7 3.2 %collective-permute-start = (bf16[128,64]{0,1:T(8,128)(2,1)S(1)}, bf16[128,64]{0,1:T(8,128)(2,1)S(1)}, u32[]{:S(2)}, u32[]{:S(2)}) collective-permute-start(bf16[128,64]{0,1:T(8,128)(2,1)S(1)} %slice.56), channel_id=1, source_target_pairs={{0,8},{8,16},{16,24},{24,32},{32,40},{40,48},{48,56},{56,64},{64,7... | collective-permute-start | bytes 49160 | tf_op jit(solution)/shard_map/ppermute | solution.py:13
  16.9 0.7 slice.63
  17.6 2.9 %collective-permute-start.2 = (bf16[128,64]{0,1:T(8,128)(2,1)S(1)}, bf16[128,64]{0,1:T(8,128)(2,1)S(1)}, u32[]{:S(2)}, u32[]{:S(2)}) collective-permute-start(bf16[128,64]{0,1:T(8,128)(2,1)S(1)} %slice.63), channel_id=1, source_target_pairs={{0,8},{8,16},{16,24},{24,32},{32,40},{40,48},{48,56},{56,64},{64,7... | collective-permute-start | bytes 49160 | tf_op jit(solution)/shard_map/ppermute | solution.py:13
  20.5 0.9 copy_bitcast_fusion
  21.4 0.9 copy_bitcast_fusion.2
  22.3 1.0 reshape.134
  23.3 0.7 pad_add_fusion
  24.7 0.9 compare_and_fusion
  25.6 0.8 copy_bitcast_fusion.1
  26.4 0.8 copy_bitcast_fusion.3
  28.4 2.1 convolution_convert_fusion
  30.4 5.8 %all-to-all-start = ((bf16[8,64,2048]{2,1,0:T(8,128)(2,1)}), bf16[8,64,2048]{2,1,0:T(8,128)(2,1)S(1)}, u32[]{:S(2)}, u32[]{:S(2)}) async-start(bf16[8,64,2048]{2,1,0:T(8,128)(2,1)} %bitcast.63), calls=%async_computation | async-start | bytes 4194304 | tf_op jit(solution)/shard_map/all_to_all | solution.py:34
  36.2 26.2 %all-to-all-done = bf16[8,64,2048]{2,1,0:T(8,128)(2,1)S(1)} async-done(((bf16[8,64,2048]{2,1,0:T(8,128)(2,1)}), bf16[8,64,2048]{2,1,0:T(8,128)(2,1)S(1)}, u32[]{:S(2)}, u32[]{:S(2)}) %all-to-all-start) | async-done | bytes 2097184 | tf_op jit(solution)/shard_map/all_to_all | solution.py:34
  62.8 1.1 fusion.22
  64.4 29.6 %all_to_all.20 = bf16[8,64,2048]{2,1,0:T(8,128)(2,1)S(1)} all-to-all(bf16[8,64,2048]{2,1,0:T(8,128)(2,1)S(1)} %broadcast_in_dim.18), channel_id=1, replica_groups=mesh['sp'=64,'tp'=8] {'tp'}, dimensions={0} | all-to-all | bytes 4194304 | tf_op jit(solution)/shard_map/all_to_all | solution.py:46
  94.0 71.6 %all-gather.2.cloned.1.call-done = bf16[2048,2112]{1,0:T(8,128)(2,1)} async-done(((bf16[32,2112]{1,0:T(8,128)(2,1)}), bf16[2048,2112]{1,0:T(8,128)(2,1)}) %all-gather.2.cloned.1.call-update) | async-done | bytes 8650768 | tf_op jit(solution)/shard_map/all_gather | solution.py:19
  165.5 4.7 %fusion.4 = f32[512,704]{0,1:T(8,128)} fusion(bf16[512,2048]{1,0:T(8,128)(2,1)S(1)} %bitcast.65, bf16[2048,2112]{1,0:T(8,128)(2,1)} %all-gather.2.cloned.1.call-done), kind=kOutput, calls=%fused_computation.6 | convolution fusion | flops 1476395008 | bytes 6684672 | tf_op jit(solution)/shard_map/dot_general | solution.py:128
  170.3 9.4 %fusion.6 = bf16[512,2048]{1,0:T(8,128)(2,1)} fusion(bf16[2048,2112]{1,0:T(8,128)(2,1)} %all-gather.2.cloned.1.call-done, bf16[512,2048]{1,0:T(8,128)(2,1)S(1)} %bitcast.66, f32[512,704]{0,1:T(8,128)} %fusion.4), kind=kOutput, calls=%fused_computation.9 | convolution fusion | flops 2956001280 | bytes 11927552 | tf_op jit(solution)/shard_map/dot_general | solution.py:133
  179.7 38.7 %all_to_all.21 = bf16[8,64,2048]{2,1,0:T(8,128)(2,1)S(1)} all-to-all(bf16[8,64,2048]{2,1,0:T(8,128)(2,1)} %bitcast.67), channel_id=1, replica_groups=mesh['sp'=64,'tp'=8] {'tp'}, dimensions={0} | all-to-all | bytes 4194304 | tf_op jit(solution)/shard_map/all_to_all | solution.py:34
  219.1 29.7 %all_to_all.22 = bf16[8,64,2048]{2,1,0:T(8,128)(2,1)S(1)} all-to-all(bf16[8,64,2048]{2,1,0:T(8,128)(2,1)S(1)} %broadcast_in_dim.19), channel_id=1, replica_groups=mesh['sp'=64,'tp'=8] {'tp'}, dimensions={0} | all-to-all | bytes 4194304 | tf_op jit(solution)/shard_map/all_to_all | solution.py:46
  248.7 1.3 copy.45
  (30 shorter events, 4.0 us)
Async XLA Ops:
  6.5 21.8 %copy-start = (bf16[128,2048]{1,0:T(8,128)(2,1)S(1)}, bf16[128,2048]{1,0:T(8,128)(2,1)}, u32[]{:S(2)}) copy-start(bf16[128,2048]{1,0:T(8,128)(2,1)} %param.17) | copy-start | bytes 1572868
  6.5 21.1 %copy-start.2 = (f32[2]{0:T(128)S(1)}, f32[2]{0:T(128)}, u32[]{:S(2)}) copy-start(f32[2]{0:T(128)} %param.15) | copy-start | bytes 28
  6.5 159.0 %all-gather.2.cloned.1.call-start = ((), (), s32[]{:S(2)}) async-start(), calls=%async_computation.4 | async-start | bytes 9052160 | tf_op jit(solution)/shard_map/all_gather | solution.py:19
  8.9 14.4 %collective-permute-start.1 = (s32[128]{0:T(128)S(1)}, s32[128]{0:T(128)S(1)}, u32[]{:S(2)}, u32[]{:S(2)}) collective-permute-start(s32[128]{0:T(128)S(1)} %slice_add_fusion), channel_id=1, source_target_pairs={{0,8},{8,16},{16,24},{24,32},{32,40},{40,48},{48,56},{56,64},{64,7... | collective-permute-start | bytes 1544 | tf_op jit(solution)/shard_map/ppermute | solution.py:13
  13.7 12.8 %collective-permute-start = (bf16[128,64]{0,1:T(8,128)(2,1)S(1)}, bf16[128,64]{0,1:T(8,128)(2,1)S(1)}, u32[]{:S(2)}, u32[]{:S(2)}) collective-permute-start(bf16[128,64]{0,1:T(8,128)(2,1)S(1)} %slice.56), channel_id=1, source_target_pairs={{0,8},{8,16},{16,24},{24,32},{32,40},{40,48},{48,56},{56,64},{64,7... | collective-permute-start | bytes 49160 | tf_op jit(solution)/shard_map/ppermute | solution.py:13
  17.6 8.0 %collective-permute-start.2 = (bf16[128,64]{0,1:T(8,128)(2,1)S(1)}, bf16[128,64]{0,1:T(8,128)(2,1)S(1)}, u32[]{:S(2)}, u32[]{:S(2)}) collective-permute-start(bf16[128,64]{0,1:T(8,128)(2,1)S(1)} %slice.63), channel_id=1, source_target_pairs={{0,8},{8,16},{16,24},{24,32},{32,40},{40,48},{48,56},{56,64},{64,7... | collective-permute-start | bytes 49160 | tf_op jit(solution)/shard_map/ppermute | solution.py:13
  30.4 32.0 %all-to-all-start = ((bf16[8,64,2048]{2,1,0:T(8,128)(2,1)}), bf16[8,64,2048]{2,1,0:T(8,128)(2,1)S(1)}, u32[]{:S(2)}, u32[]{:S(2)}) async-start(bf16[8,64,2048]{2,1,0:T(8,128)(2,1)} %bitcast.63), calls=%async_computation | async-start | bytes 4194304 | tf_op jit(solution)/shard_map/all_to_all | solution.py:34
  36.2 27.7 %copy-start.1 = (f32[2048]{0:T(1024)S(1)}, f32[2048]{0:T(1024)}, u32[]{:S(2)}) copy-start(f32[2048]{0:T(1024)} %param.18) | copy-start | bytes 24580
Sparse Core Ops, SparseCore 0:
  10.3 155.2 all-gather.1
where the time goes:
time: 258 us; the launch traced here: 257 us
  blocking collectives  97.9 us (38%)
  waiting for transfers between devices  97.8 us (38%)
  matrix products  16.9 us (7%)
  starting transfers between devices  15.9 us (6%)
  between operations  13.6 us (5%)
  local copies, waits for them, and re-layouts  7.79 us (3%)
  other arithmetic  6.98 us (3%)
    all_gather x1, waiting for transfers between devices, gather_turned(): lax.all_gather(both, axis, axis=0, tiled=True)  71.6 us
    all_to_all x2, blocking collectives, sent_to_all(): lax.all_to_all(jnp.broadcast_to(shard[None], (size, *shard.shape)), axis,...  59.2 us
    all_to_all x1, blocking collectives, sum_at_owner(): lax.all_to_all(pieces, axis, split_axis=0, concat_axis=0, tiled=True)  38.7 us
    all_to_all x1, waiting for transfers between devices, sum_at_owner(): lax.all_to_all(pieces, axis, split_axis=0, concat_axis=0, tiled=True)  26.2 us
    ppermute x3, starting transfers between devices, from_behind(): return lax.ppermute(shard, axis, pairs)  10.1 us
    dot_general x1, matrix products, on_device(): jnp.dot(picked, down_whole, preferred_element_type=jnp.float32)  9.43 us
    all_to_all x1, starting transfers between devices, sum_at_owner(): lax.all_to_all(pieces, axis, split_axis=0, concat_axis=0, tiled=True)  5.81 us
  transfers between devices with their start and end apart: 5, of which 2 were waited for; matrix products, arithmetic and copies ran while one was open for 5% of the time, Pallas kernels for 0%

commit v1 on v0

--- a/solution.py
+++ b/solution.py
@@ -16,7 +16,13 @@
 def gather_turned(arrays, axis, dims):
     turned = [jnp.moveaxis(a, dim, 0) for a, dim in zip(arrays, dims)]
     both = jnp.concatenate([t.reshape(len(t), -1) for t in turned], axis=1)
-    result, at, finished = (lax.all_gather(both, axis, axis=0, tiled=True), 0, [])
+    result, at, finished = (
+        jnp.concatenate(
+            lax.all_to_all(jnp.stack([both] * lax.axis_size(axis)), axis, 0, 0), axis=0
+        ),
+        0,
+        [],
+    )
     for t, dim in zip(turned, dims):
         slab = result[:, at : at + t[0].size].reshape(-1, *t.shape[1:])
         finished.append(jnp.moveaxis(slab, 0, dim))

time: 258 us -> 577 us (2.24)
  blocking collectives: 97.9 us -> 470 us
  waiting for transfers between devices: 97.8 us -> 52.3 us
  between operations: 13.6 us -> 0.22 us
    all_to_all x0 -> x1, blocking collectives: none -> 407 us  [gather_turned(): lax.all_to_all(jnp.stack([both] * lax.axis_size(axis)), axis, 0, 0)]
    all_gather x1 -> x0, waiting for transfers between devices: 71.6 us -> none  [gather_turned(): lax.all_gather(both, axis, axis=0, tiled=True)]
    all_to_all x2 -> x1, blocking collectives: 59.2 us -> 29.7 us  [sent_to_all(): lax.all_to_all(jnp.broadcast_to(shard[None], (size, *shard.shape)), axis,...]
    all_to_all x0 -> x1, waiting for transfers between devices: none -> 26.1 us  [sent_to_all(): lax.all_to_all(jnp.broadcast_to(shard[None], (size, *shard.shape)), axis,...]
  transfers between devices with their start and end apart: 5 -> 5, of which waited for: 2 -> 2; matrix products, arithmetic and copies ran while one was open for 5% -> 1% of each run, Pallas kernels for 0% -> 0%
where the time goes in v1:
time: 577 us; the launch traced here: 576 us
  blocking collectives  470 us (81%)
  waiting for transfers between devices  52.3 us (9%)
  starting transfers between devices  20.5 us (4%)
  matrix products  15 us (3%)
  local copies, waits for them, and re-layouts  11.7 us (2%)
  other arithmetic  6.18 us (1%)
    all_to_all x1, blocking collectives, gather_turned(): lax.all_to_all(jnp.stack([both] * lax.axis_size(axis)), axis, 0, 0)  407 us
    all_to_all x1, blocking collectives, sum_at_owner(): lax.all_to_all(pieces, axis, split_axis=0, concat_axis=0, tiled=True)  33.7 us
    all_to_all x1, blocking collectives, sent_to_all(): lax.all_to_all(jnp.broadcast_to(shard[None], (size, *shard.shape)), axis,...  29.7 us
    all_to_all x1, waiting for transfers between devices, sum_at_owner(): lax.all_to_all(pieces, axis, split_axis=0, concat_axis=0, tiled=True)  26.2 us
    all_to_all x1, waiting for transfers between devices, sent_to_all(): lax.all_to_all(jnp.broadcast_to(shard[None], (size, *shard.shape)), axis,...  26.1 us
  transfers between devices with their start and end apart: 5, of which 2 were waited for; matrix products, arithmetic and copies ran while one was open for 1% of the time, Pallas kernels for 0%

profile of v1, /device:TPU:1, one launch (start us, length us, event | category | flops | bytes accessed | tf_op | source)
XLA Modules:
  0.0 576.0 jit_solution(7722270333320070947)
XLA Ops:
  0.0 0.8 slice.63
  0.8 4.0 collective-permute-start.2
  5.5 3.2 collective-permute-start.1
  8.7 0.7 slice.56
  9.4 2.9 collective-permute-start
  12.3 0.9 copy_bitcast_fusion
  13.2 0.9 copy_bitcast_fusion.2
  14.1 1.0 reshape.140
  16.6 0.9 compare_and_fusion
  17.5 0.8 copy_bitcast_fusion.1
  19.4 2.0 convolution_convert_fusion
  21.5 5.8 %all-to-all-start = ((bf16[8,64,2048]{2,1,0:T(8,128)(2,1)}), bf16[8,64,2048]{2,1,0:T(8,128)(2,1)S(1)}, u32[]{:S(2)}, u32[]{:S(2)}) async-start(bf16[8,64,2048]{2,1,0:T(8,128)(2,1)} %bitcast.66), calls=%async_computation | async-start | bytes 4194304 | tf_op jit(solution)/shard_map/all_to_all | solution.py:40
  27.3 26.2 %all-to-all-done = bf16[8,64,2048]{2,1,0:T(8,128)(2,1)S(1)} async-done(((bf16[8,64,2048]{2,1,0:T(8,128)(2,1)}), bf16[8,64,2048]{2,1,0:T(8,128)(2,1)S(1)}, u32[]{:S(2)}, u32[]{:S(2)}) %all-to-all-start) | async-done | bytes 2097184 | tf_op jit(solution)/shard_map/all_to_all | solution.py:40
  53.9 1.1 fusion.22
  55.2 1.6 broadcast_in_dim.18
  56.8 4.6 all-to-all-start.1
  61.5 26.1 %all-to-all-done.1 = bf16[8,64,2048]{2,1,0:T(8,128)(2,1)S(1)} async-done(((bf16[8,64,2048]{2,1,0:T(8,128)(2,1)}), bf16[8,64,2048]{2,1,0:T(8,128)(2,1)S(1)}, u32[]{:S(2)}, u32[]{:S(2)}) %all-to-all-start.1) | async-done | bytes 2097184 | tf_op jit(solution)/shard_map/all_to_all | solution.py:52
  88.2 406.7 %all_to_all.25 = bf16[64,32,2112]{2,1,0:T(8,128)(2,1)S(1)} all-to-all(bf16[64,32,2112]{2,1,0:T(8,128)(2,1)S(1)} %stack.2), channel_id=1, replica_groups=mesh['sp'=64,'tp'=8] {'sp'}, dimensions={0} | all-to-all | bytes 17301504 | tf_op jit(solution)/shard_map/all_to_all | solution.py:21
  494.9 3.4 copy-done.1
  498.3 2.8 fusion.4
  501.2 9.4 %fusion.6 = bf16[512,2048]{1,0:T(8,128)(2,1)} fusion(bf16[2048,2112]{1,0:T(8,128)(2,1)} %bitcast.65, bf16[512,2048]{1,0:T(8,128)(2,1)S(1)} %bitcast.69, f32[512,704]{0,1:T(8,128)} %fusion.4), kind=kOutput, calls=%fused_computation.9 | convolution fusion | flops 2956001280 | bytes 11927552 | tf_op jit(solution)/shard_map/dot_general | solution.py:139
  510.6 33.7 %all_to_all.26 = bf16[8,64,2048]{2,1,0:T(8,128)(2,1)S(1)} all-to-all(bf16[8,64,2048]{2,1,0:T(8,128)(2,1)} %bitcast.70), channel_id=1, replica_groups=mesh['sp'=64,'tp'=8] {'tp'}, dimensions={0} | all-to-all | bytes 4194304 | tf_op jit(solution)/shard_map/all_to_all | solution.py:40
  545.0 29.7 %all_to_all.27 = bf16[8,64,2048]{2,1,0:T(8,128)(2,1)S(1)} all-to-all(bf16[8,64,2048]{2,1,0:T(8,128)(2,1)S(1)} %broadcast_in_dim.19), channel_id=1, replica_groups=mesh['sp'=64,'tp'=8] {'tp'}, dimensions={0} | all-to-all | bytes 4194304 | tf_op jit(solution)/shard_map/all_to_all | solution.py:52
  574.7 1.3 copy.45
  (40 shorter events, 5.1 us)
Async XLA Ops:
  0.0 19.4 %copy-start = (bf16[128,2048]{1,0:T(8,128)(2,1)S(1)}, bf16[128,2048]{1,0:T(8,128)(2,1)}, u32[]{:S(2)}) copy-start(bf16[128,2048]{1,0:T(8,128)(2,1)} %param.17) | copy-start | bytes 1572868
  0.0 19.0 %copy-start.2 = (bf16[512,64]{0,1:T(8,128)(2,1)S(1)}, bf16[512,64]{0,1:T(8,128)(2,1)}, u32[]{:S(2)}) copy-start(bf16[512,64]{0,1:T(8,128)(2,1)} %param.13) | copy-start | bytes 196612
  0.0 18.6 %copy-start.7 = (f32[2]{0:T(128)S(1)}, f32[2]{0:T(128)}, u32[]{:S(2)}) copy-start(f32[2]{0:T(128)} %param.15) | copy-start | bytes 28
  0.8 16.6 %collective-permute-start.2 = (bf16[128,64]{0,1:T(8,128)(2,1)S(1)}, bf16[128,64]{0,1:T(8,128)(2,1)S(1)}, u32[]{:S(2)}, u32[]{:S(2)}) collective-permute-start(bf16[128,64]{0,1:T(8,128)(2,1)S(1)} %slice.63), channel_id=1, source_target_pairs={{0,8},{8,16},{16,24},{24,32},{32,40},{40,48},{48,56},{56,64},{64,7... | collective-permute-start | bytes 49160 | tf_op jit(solution)/shard_map/ppermute | solution.py:13
  5.5 9.7 %collective-permute-start.1 = (s32[128]{0:T(128)S(1)}, s32[128]{0:T(128)S(1)}, u32[]{:S(2)}, u32[]{:S(2)}) collective-permute-start(s32[128]{0:T(128)S(1)} %slice_add_fusion), channel_id=1, source_target_pairs={{0,8},{8,16},{16,24},{24,32},{32,40},{40,48},{48,56},{56,64},{64,7... | collective-permute-start | bytes 1544 | tf_op jit(solution)/shard_map/ppermute | solution.py:13
  9.4 9.5 %collective-permute-start = (bf16[128,64]{0,1:T(8,128)(2,1)S(1)}, bf16[128,64]{0,1:T(8,128)(2,1)S(1)}, u32[]{:S(2)}, u32[]{:S(2)}) collective-permute-start(bf16[128,64]{0,1:T(8,128)(2,1)S(1)} %slice.56), channel_id=1, source_target_pairs={{0,8},{8,16},{16,24},{24,32},{32,40},{40,48},{48,56},{56,64},{64,7... | collective-permute-start | bytes 49160 | tf_op jit(solution)/shard_map/ppermute | solution.py:13
  21.5 32.0 %all-to-all-start = ((bf16[8,64,2048]{2,1,0:T(8,128)(2,1)}), bf16[8,64,2048]{2,1,0:T(8,128)(2,1)S(1)}, u32[]{:S(2)}, u32[]{:S(2)}) async-start(bf16[8,64,2048]{2,1,0:T(8,128)(2,1)} %bitcast.66), calls=%async_computation | async-start | bytes 4194304 | tf_op jit(solution)/shard_map/all_to_all | solution.py:40
  27.3 27.7 %copy-start.6 = (f32[2048]{0:T(1024)S(1)}, f32[2048]{0:T(1024)}, u32[]{:S(2)}) copy-start(f32[2048]{0:T(1024)} %param.18) | copy-start | bytes 24580
  56.7 4.6 copy-start.3
  56.7 4.6 copy-start.4
  56.7 4.6 copy-start.5
  56.8 30.8 %all-to-all-start.1 = ((bf16[8,64,2048]{2,1,0:T(8,128)(2,1)}), bf16[8,64,2048]{2,1,0:T(8,128)(2,1)S(1)}, u32[]{:S(2)}, u32[]{:S(2)}) async-start(bf16[8,64,2048]{2,1,0:T(8,128)(2,1)} %broadcast_in_dim.18), calls=%async_computation.1 | async-start | bytes 4194304 | tf_op jit(solution)/shard_map/all_to_all | solution.py:52
  494.9 3.4 copy-start.1
